TPU v7x, 512 devices: a whole 4x8x8 slice. The times are simulated.
512 devices in a mesh: ep: 32 (over z, x), tp: 16 (over y, core).
Axes of the slice: x: 4, y: 8, z: 8, core: 2. Of those that a mesh axis runs over, the one named last changes fastest.
Arguments:
- pool_input: bfloat16 [8192, 2048], P('ep', 'tp'), may hold values from -6 to 6
- pool_map: bfloat16 [16, 128, 128], replicated, may hold values from -0.5 to 0.5
- pool_scale: float32 [2048], replicated, may hold values from 0.1 to 1.9
- out_proj: bfloat16 [2048, 4096], P('tp'), may hold values from -0.125 to 0.125
- moe_input: bfloat16 [4096, 4096], P('ep'), may hold values from -6 to 6
- norm_gain: float32 [4096], replicated, may hold values from 0.1 to 1.9
- routes: int32 [4096, 4], P('ep'), may hold values from 0 to 31, all different within a row; in each aligned block of 128 rows (0 to 127, 128 to 255, ...) at most 24 rows name the same one
- route_weights: float32 [4096, 4], P('ep'), may hold values from 0.1 to 1
- expert_gate: bfloat16 [32, 4096, 1024], P('ep', None, 'tp'), may hold values from -0.09375 to 0.09375
- expert_up: bfloat16 [32, 4096, 1024], P('ep', None, 'tp'), may hold values from -0.09375 to 0.09375
- expert_down: bfloat16 [32, 1024, 4096], P('ep', None, 'tp'), may hold values from -0.1875 to 0.1875
- shared_gate: bfloat16 [4096, 512], P(None, 'tp'), may hold values from -0.09375 to 0.09375
- shared_up: bfloat16 [4096, 512], P(None, 'tp'), may hold values from -0.09375 to 0.09375
- shared_down: bfloat16 [512, 4096], P('tp'), may hold values from -0.25 to 0.25
Outputs:
- mixer_output: bfloat16 [8192, 4096], P('ep', 'tp')
- moe_output: bfloat16 [4096, 4096], P('ep', 'tp')
Inputs may be any that keep to these rules, and one draw needn't show every extreme that they name: `routes`: each row names 4 different experts. In each aligned block of 128 rows no expert is named by more than 24 rows, a bound that some block reaches.
All inputs are finite; a program needn't handle non-finite values.
Results may differ from a plain program's by a relative error of at most 0.017.
Values may be sent and summed in bfloat16 or wider, within the bound.
No kernel may reach another device: no remote copies, remote signals or barrier semaphores. Data moves between devices by JAX's collectives and lax.ppermute only.
A program may use at most 64 MiB of HBM per device.

v0:
```python
import jax
import jax.numpy as jnp
from jax import lax
from jax.sharding import PartitionSpec as P

windows = (2, 4, 8, 16)
reach_back = 15
eps = 1e-05


def passed_along(block, axis, distance):
    devices = range(lax.axis_size(axis))
    route = [(i - distance, i) for i in devices if i - distance in devices]
    return lax.ppermute(block, axis, route)


def sent_to_all(x, axis):
    devices = lax.axis_size(axis)
    return lax.all_to_all(jnp.broadcast_to(x[None], (devices, *x.shape)), axis, 0, 0, tiled=True)


def joined_along(pieces, dim):
    shape = list(pieces.shape[1:])
    shape[dim] *= pieces.shape[0]
    return jnp.moveaxis(pieces, 0, dim).reshape(shape)


def gathered_copies(x, axis, dim):
    pieces = sent_to_all(x, axis)
    return joined_along(pieces, dim)


def in_one_piece(arrays, axis, dim, along):
    both = jnp.concatenate(arrays, axis=along)
    out, at, done = (lax.psum_scatter(both, axis, scatter_dimension=dim, tiled=True), 0, [])
    for a in arrays:
        done.append(lax.slice_in_dim(out, at, at + a.shape[along], axis=along))
        at += a.shape[along]
    return tuple(done)


def pool_branch(pool_input, pool_map, pool_scale, out_proj):
    row_count = pool_input.shape[0]
    channels = pool_input.shape[1]
    group_dim = pool_map.shape[1]
    local_groups = channels // group_dim
    tp_rank = lax.axis_index("tp")
    ep_rank = lax.axis_index("ep")
    earlier_rows = passed_along(pool_input[row_count - reach_back :], "ep", 1)
    values = pool_input.astype(jnp.float32)
    extended = jnp.concatenate([earlier_rows.astype(jnp.float32), values], axis=0)
    position = (ep_rank * row_count + jnp.arange(row_count, dtype=jnp.int32)).astype(jnp.float32)
    group_ids = tp_rank * local_groups + jnp.arange(channels, dtype=jnp.int32) // group_dim
    group_kind = group_ids % 4
    running = jnp.zeros((row_count, channels), jnp.float32)
    pooled = -values
    for lag_step in range(reach_back + 1):
        running = running + extended[reach_back - lag_step : reach_back - lag_step + row_count]
        if lag_step + 1 in windows:
            kind_id = windows.index(lag_step + 1)
            counts = jnp.minimum(position + 1.0, float(lag_step + 1))
            select = (group_kind == kind_id).astype(jnp.float32)
            pooled = pooled + select[None, :] * running / counts[:, None]
    pooled = pooled.astype(jnp.bfloat16)
    my_maps = lax.dynamic_slice_in_dim(pool_map, tp_rank * local_groups, local_groups, 0)
    my_scale = lax.dynamic_slice_in_dim(pool_scale, tp_rank * channels, channels, 0)
    mapped = jnp.einsum(
        "rgc,gcd->rgd",
        pooled.reshape(row_count, local_groups, group_dim),
        my_maps,
        preferred_element_type=jnp.float32,
    )
    group_out = (mapped.reshape(row_count, channels) * my_scale[None, :]).astype(jnp.bfloat16)
    return jnp.dot(group_out, out_proj, preferred_element_type=jnp.float32)


def dispatch_rows(routes, expert_count, capacity):
    tok_count, top_count = routes.shape
    flat_ids = routes.reshape(tok_count * top_count)
    one_hot = (flat_ids[:, None] == jnp.arange(expert_count, dtype=jnp.int32)[None, :]).astype(
        jnp.int32
    )
    earlier = jnp.cumsum(one_hot, axis=0) - one_hot
    slot_ids = jnp.sum(earlier * one_hot, axis=1)
    return (flat_ids * capacity + slot_ids).reshape(tok_count, top_count)


def per_device(
    pool_input,
    pool_map,
    pool_scale,
    out_proj,
    moe_input,
    norm_gain,
    routes,
    route_weights,
    expert_gate,
    expert_up,
    expert_down,
    shared_gate,
    shared_up,
    shared_down,
):
    mixer_part = pool_branch(pool_input, pool_map, pool_scale, out_proj)
    values = moe_input.astype(jnp.float32)
    centre = values - jnp.mean(values, axis=1, keepdims=True)
    variance = jnp.mean(centre * centre, axis=1, keepdims=True)
    normed = (centre * lax.rsqrt(variance + eps) * norm_gain[None, :]).astype(jnp.bfloat16)
    expert_count = lax.axis_size("ep")
    tok_count = moe_input.shape[0]
    top_count = routes.shape[1]
    capacity = (3 * tok_count * top_count + 2 * expert_count - 1) // (2 * expert_count)
    slot_index = dispatch_rows(routes, expert_count, capacity)
    buffer_len = expert_count * capacity
    targets = jnp.arange(buffer_len, dtype=jnp.int32)[:, None]
    placing = jnp.zeros((buffer_len, tok_count), jnp.float32)
    for top_step in range(top_count):
        placing = placing + (targets == slot_index[None, :, top_step]).astype(jnp.float32)
    outgoing = jnp.dot(
        placing.astype(jnp.bfloat16), normed, preferred_element_type=jnp.float32
    ).astype(jnp.bfloat16)
    gate_weight = expert_gate[0]
    up_weight = expert_up[0]
    down_weight = expert_down[0]
    tp_rank = lax.axis_index("tp")
    slice_width = outgoing.shape[1] // lax.axis_size("tp")
    my_slice = lax.dynamic_slice_in_dim(outgoing, tp_rank * slice_width, slice_width, 1)
    arrived = lax.all_to_all(my_slice, "ep", split_axis=0, concat_axis=0, tiled=True)
    shard_cols = lax.all_gather(arrived, "tp", axis=1, tiled=True)
    gate_val = jnp.dot(shard_cols, gate_weight, preferred_element_type=jnp.float32)
    up_val = jnp.dot(shard_cols, up_weight, preferred_element_type=jnp.float32)
    hidden = (jax.nn.silu(gate_val) * up_val).astype(jnp.bfloat16)
    expert_result = jnp.dot(
        gathered_copies(hidden, "tp", 1), down_weight, preferred_element_type=jnp.float32
    ).astype(jnp.bfloat16)
    returned = lax.all_to_all(expert_result, "ep", split_axis=0, concat_axis=0, tiled=True)
    routed = jnp.zeros((tok_count, returned.shape[1]), jnp.float32)
    for top_step in range(top_count):
        picked = returned[slot_index[:, top_step]].astype(jnp.float32)
        routed = routed + route_weights[:, top_step, None] * picked
    shared_gate_val = jnp.dot(normed, shared_gate, preferred_element_type=jnp.float32)
    shared_up_val = jnp.dot(normed, shared_up, preferred_element_type=jnp.float32)
    shared_hidden = (jax.nn.silu(shared_gate_val) * shared_up_val).astype(jnp.bfloat16)
    shared_part = jnp.dot(shared_hidden, shared_down, preferred_element_type=jnp.float32)
    mixer_sum, shared_sum = tuple(
        (
            part.astype(jnp.float32)
            for part in in_one_piece(
                (mixer_part.astype(jnp.bfloat16), shared_part.astype(jnp.bfloat16)), "tp", 1, 0
            )
        )
    )
    return (mixer_sum.astype(jnp.bfloat16), (routed + shared_sum).astype(jnp.bfloat16))


def solution(mesh):
    return jax.shard_map(
        per_device,
        mesh=mesh,
        in_specs=(
            P("ep", "tp"),
            P(),
            P(),
            P("tp", None),
            P("ep", None),
            P(),
            P("ep", None),
            P("ep", None),
            P("ep", None, "tp"),
            P("ep", None, "tp"),
            P("ep", None, "tp"),
            P(None, "tp"),
            P(None, "tp"),
            P("tp", None),
        ),
        out_specs=(P("ep", "tp"), P("ep", "tp")),
        check_vma=False,
    )
```

profile of v0, /device:TPU:1, one launch (start us, length us, event | category | flops | bytes accessed | tf_op | source)
XLA Modules:
  0.0 197.1 jit_solution(10955667984421792337)
XLA Ops:
  7.2 0.9 copy.27
  8.4 1.2 reduce-window.6
  10.8 1.5 convert_reduce_fusion
  12.8 1.9 fusion.13
  14.8 27.4 %all_to_all.29 = bf16[32,24,256]{2,1,0:T(8,128)(2,1)} all-to-all(bf16[32,24,256]{2,1,0:T(8,128)(2,1)S(1)} %bitcast.88), channel_id=1, replica_groups=mesh['ep'=32,'tp'=16] {'ep'}, dimensions={0} | all-to-all | bytes 786432 | tf_op jit(solution)/shard_map/all_to_all | solution.py:128
  42.3 2.3 %collective-permute-start = (bf16[15,128]{1,0:T(8,128)(2,1)S(1)}, bf16[15,128]{1,0:T(8,128)(2,1)S(1)}, u32[]{:S(2)}, u32[]{:S(2)}) collective-permute-start(bf16[15,128]{1,0:T(8,128)(2,1)S(1)} %slice.88), channel_id=1, source_target_pairs={{0,16},{16,32},{32,48},{48,64},{64,80},{80,96},{96,112},{112,128},... | collective-permute-start | bytes 11528 | tf_op jit(solution)/shard_map/ppermute | solution.py:14
  45.7 2.4 %convolution_convert_fusion.1 = bf16[128,4096]{1,0:T(8,128)(2,1)S(1)} fusion(bf16[32,4096]{1,0:T(8,128)(2,1)S(1)} %copy-done.5, bf16[4096,32]{0,1:T(8,128)(2,1)} %param.26, f32[128,32]{0,1:T(8,128)S(1)} %fusion.102, bf16[128,4096]{1,0:T(8,128)(2,1)S(1)} %copy-done.2, f32[4096]{0:T(1024)S(1)} %copy-done.7, f32[128]{0:T(128)S(1)} %add_rsqrt_fusion, ...), kind=kOutput, calls=%fused_computation.5 | convolution fusion | flops 70279168 | bytes 2655232 | tf_op jit(solution)/shard_map/dot_general | solution.py:144
  48.2 0.8 dynamic_slice.10
  49.0 3.3 %convolution_convert_fusion = bf16[256,4096]{1,0:T(8,128)(2,1)} fusion(bf16[128,4096]{1,0:T(8,128)(2,1)S(1)} %copy-done, f32[256,128]{1,0:T(8,128)S(1)} %convert_element_type.122, f32[15,128]{1,0:T(8,128)S(1)} %convert_element_type.124, f32[128]{0:T(128)S(1)} %dynamic_slice.10, f32[256]{0:T(256)S(1)} %get-tuple-element.18, f32[128]{0:T(128)} %get-tuple-element.14, ...), kind=kOutput, calls=%fused_computation.4 | convolution fusion | flops 279379968 | bytes 3323908 | tf_op jit(solution)/shard_map/dot_general | solution.py:74
  52.2 3.6 %pad_maximum_fusion = bf16[384,4096]{1,0:T(8,128)(2,1)} fusion(bf16[128,4096]{1,0:T(8,128)(2,1)S(1)} %convolution_convert_fusion.1, bf16[256,4096]{1,0:T(8,128)(2,1)} %convolution_convert_fusion), kind=kLoop, calls=%fused_computation.6 | loop fusion | flops 6291456 | bytes 6291456 | tf_op jit(solution)/shard_map/concatenate | solution.py:34
  55.8 44.0 %all-gather.2.cloned.1.call-done = bf16[768,4096]{1,0:T(8,128)(2,1)} async-done(((bf16[768,256]{1,0:T(8,128)(2,1)}), bf16[768,4096]{1,0:T(8,128)(2,1)}) %all-gather.2.cloned.1.call-update) | async-done | bytes 6291472 | tf_op jit(solution)/shard_map/all_gather | solution.py:129
  99.8 5.0 %fusion.11 = f32[768,64]{0,1:T(8,128)S(1)} fusion(bf16[768,4096]{1,0:T(8,128)(2,1)} %all-gather.2.cloned.1.call-done, bf16[1,4096,64]{1,2,0:T(8,128)(2,1)S(1)} %copy-done.4), kind=kOutput, calls=%fused_computation.39 | convolution fusion | flops 402653184 | bytes 7012352 | tf_op jit(solution)/shard_map/dot_general | solution.py:130
  104.8 2.1 %fusion.5 = bf16[768,64]{0,1:T(8,128)(2,1)S(1)} fusion(bf16[768,4096]{1,0:T(8,128)(2,1)S(1)} %copy-done.1, bf16[1,4096,64]{1,2,0:T(8,128)(2,1)S(1)} %copy-done.3, f32[768,64]{0,1:T(8,128)S(1)} %fusion.11), kind=kOutput, calls=%fused_computation.16 | convolution fusion | flops 402948096 | bytes 7110656 | tf_op jit(solution)/shard_map/dot_general | solution.py:131
  107.0 52.2 %all_to_all.30 = bf16[16,768,64]{1,2,0:T(8,128)(2,1)S(1)} all-to-all(bf16[16,768,64]{1,2,0:T(8,128)(2,1)S(1)} %broadcast_in_dim.2), channel_id=1, replica_groups=mesh['ep'=32,'tp'=16] {'tp'}, dimensions={0} | all-to-all | bytes 3145728 | tf_op jit(solution)/shard_map/all_to_all | solution.py:19
  159.3 1.4 convolution_convert_fusion.2
  160.6 9.9 %all-to-all-start.2 = ((bf16[32,24,256]{2,1,0:T(8,128)(2,1)}), bf16[32,24,256]{2,1,0:T(8,128)(2,1)S(1)}, u32[]{:S(2)}, u32[]{:S(2)}) async-start(bf16[32,24,256]{2,1,0:T(8,128)(2,1)} %bitcast.17), calls=%async_computation.3 | async-start | bytes 786432 | tf_op jit(solution)/shard_map/all_to_all | solution.py:136
  170.6 11.8 %reduce-scatter.2.cloned.1.call-done = bf16[384,256]{1,0:T(8,128)(2,1)} async-done(((bf16[384,4096]{1,0:T(8,128)(2,1)}), bf16[384,256]{1,0:T(8,128)(2,1)}) %reduce-scatter.2.cloned.1.call-update) | async-done | bytes 196624 | tf_op jit(solution)/shard_map/reduce_scatter | solution.py:35
  182.4 1.6 slice.152
  183.9 1.3 all-to-all-done.2
  185.2 0.8 gather_fusion
  186.1 0.8 gather_fusion.1
  186.9 0.8 gather_fusion.2
  187.8 0.8 gather_fusion.3
  188.6 1.6 add_convert_fusion.2
  (54 shorter events, 3.4 us)
Async XLA Ops:
  7.2 41.8 %copy-start = (bf16[128,4096]{1,0:T(8,128)(2,1)S(1)}, bf16[128,4096]{1,0:T(8,128)(2,1)}, u32[]{:S(2)}) copy-start(bf16[128,4096]{1,0:T(8,128)(2,1)} %param.17) | copy-start | bytes 3145732
  7.2 5.1 %copy-start.2 = (bf16[128,4096]{1,0:T(8,128)(2,1)S(1)}, bf16[128,4096]{1,0:T(8,128)(2,1)}, u32[]{:S(2)}) copy-start(bf16[128,4096]{1,0:T(8,128)(2,1)} %param.18) | copy-start | bytes 3145732
  7.2 5.6 %copy-start.7 = (f32[4096]{0:T(1024)S(1)}, f32[4096]{0:T(1024)}, u32[]{:S(2)}) copy-start(f32[4096]{0:T(1024)} %param.19) | copy-start | bytes 49156
  7.2 92.6 %all-gather.2.cloned.1.call-start = ((), (), s32[]{:S(2)}) async-start(), calls=%async_computation.5 | async-start | bytes 6684672 | tf_op jit(solution)/shard_map/all_gather | solution.py:129
  12.8 29.6 %copy-start.6 = (bf16[256,128]{1,0:T(8,128)(2,1)S(1)}, bf16[256,128]{1,0:T(8,128)(2,1)}, u32[]{:S(2)}) copy-start(bf16[256,128]{1,0:T(8,128)(2,1)} %param.14) | copy-start | bytes 196612
  12.8 32.4 %copy-start.10 = (bf16[4096,32]{0,1:T(8,128)(2,1)S(1)}, bf16[4096,32]{0,1:T(8,128)(2,1)}, u32[]{:S(2)}) copy-start(bf16[4096,32]{0,1:T(8,128)(2,1)} %param.25) | copy-start | bytes 786436
  14.7 31.0 %copy-start.5 = (bf16[32,4096]{1,0:T(8,128)(2,1)S(1)}, bf16[32,4096]{1,0:T(8,128)(2,1)}, u32[]{:S(2)}) copy-start(bf16[32,4096]{1,0:T(8,128)(2,1)} %param.27) | copy-start | bytes 786436
  42.3 140.1 %reduce-scatter.2.cloned.1.call-start = ((), (), s32[]{:S(2)}) async-start(), calls=%async_computation.4 | async-start | bytes 3342336 | tf_op jit(solution)/shard_map/reduce_scatter | solution.py:35
  42.3 6.6 %collective-permute-start = (bf16[15,128]{1,0:T(8,128)(2,1)S(1)}, bf16[15,128]{1,0:T(8,128)(2,1)S(1)}, u32[]{:S(2)}, u32[]{:S(2)}) collective-permute-start(bf16[15,128]{1,0:T(8,128)(2,1)S(1)} %slice.88), channel_id=1, source_target_pairs={{0,16},{16,32},{32,48},{48,64},{64,80},{80,96},{96,112},{112,128},... | collective-permute-start | bytes 11528 | tf_op jit(solution)/shard_map/ppermute | solution.py:14
  55.8 44.0 %copy-start.4 = (bf16[1,4096,64]{1,2,0:T(8,128)(2,1)S(1)}, bf16[1,4096,64]{1,2,0:T(8,128)(2,1)}, u32[]{:S(2)}) copy-start(bf16[1,4096,64]{1,2,0:T(8,128)(2,1)} %param.22) | copy-start | bytes 1572868
  55.8 48.9 %copy-start.3 = (bf16[1,4096,64]{1,2,0:T(8,128)(2,1)S(1)}, bf16[1,4096,64]{1,2,0:T(8,128)(2,1)}, u32[]{:S(2)}) copy-start(bf16[1,4096,64]{1,2,0:T(8,128)(2,1)} %param.23) | copy-start | bytes 1572868
  99.8 5.0 %copy-start.1 = (bf16[768,4096]{1,0:T(8,128)(2,1)S(1)}, bf16[768,4096]{1,0:T(8,128)(2,1)}, u32[]{:S(2)}) copy-start(bf16[768,4096]{1,0:T(8,128)(2,1)} %all-gather.2.cloned.1.call-done) | copy-start | bytes 18874372
  106.9 52.4 %copy-start.9 = (bf16[1,1024,256]{2,1,0:T(8,128)(2,1)S(1)}, bf16[1,1024,256]{2,1,0:T(8,128)(2,1)}, u32[]{:S(2)}) copy-start(bf16[1,1024,256]{2,1,0:T(8,128)(2,1)} %param.24) | copy-start | bytes 1572868
  159.3 11.3 %copy-start.8 = (f32[128,4]{0,1:T(4,128)S(1)}, f32[128,4]{0,1:T(4,128)}, u32[]{:S(2)}) copy-start(f32[128,4]{0,1:T(4,128)} %param.21) | copy-start | bytes 6148
  160.6 24.6 %all-to-all-start.2 = ((bf16[32,24,256]{2,1,0:T(8,128)(2,1)}), bf16[32,24,256]{2,1,0:T(8,128)(2,1)S(1)}, u32[]{:S(2)}, u32[]{:S(2)}) async-start(bf16[32,24,256]{2,1,0:T(8,128)(2,1)} %bitcast.17), calls=%async_computation.3 | async-start | bytes 786432 | tf_op jit(solution)/shard_map/all_to_all | solution.py:136
Sparse Core Ops, SparseCore 0:
  42.4 57.3 all-gather.1
  102.7 79.6 reduce-scatter.1
where the time goes:
time: 198 us; the launch traced here: 197 us
  blocking collectives  79.7 us (40%)
  waiting for transfers between devices  57.1 us (29%)
  matrix products  16.5 us (8%)
  between operations  14.3 us (7%)
  starting transfers between devices  12.3 us (6%)
  other arithmetic  9.7 us (5%)
  local copies, waits for them, and re-layouts  7.53 us (4%)
    all_to_all x1, blocking collectives, sent_to_all(): lax.all_to_all(jnp.broadcast_to(x[None], (devices, *x.shape)), axis, 0, 0...  52.2 us
    all_gather x1, waiting for transfers between devices, per_device(): shard_cols = lax.all_gather(arrived, 'tp', axis=1, tiled=True)  44 us
    all_to_all x1, blocking collectives, per_device(): lax.all_to_all(my_slice, 'ep', split_axis=0, concat_axis=0, tiled=True)  27.4 us
    reduce_scatter x1, waiting for transfers between devices, in_one_piece(): lax.psum_scatter(both, axis, scatter_dimension=dim, tiled=True)  11.8 us
    all_to_all x1, starting transfers between devices, per_device(): lax.all_to_all(expert_result, 'ep', split_axis=0, concat_axis=0, tiled=True)  9.89 us
    dot_general x1, matrix products, per_device(): jnp.dot(shard_cols, gate_weight, preferred_element_type=jnp.float32)  4.96 us
  transfers between devices with their start and end apart: 4, of which 3 were waited for; matrix products, arithmetic and copies ran while one was open for 11% of the time, Pallas kernels for 0%

commit v1 on v0

--- a/solution.py
+++ b/solution.py
@@ -126,7 +126,9 @@
     slice_width = outgoing.shape[1] // lax.axis_size("tp")
     my_slice = lax.dynamic_slice_in_dim(outgoing, tp_rank * slice_width, slice_width, 1)
     arrived = lax.all_to_all(my_slice, "ep", split_axis=0, concat_axis=0, tiled=True)
-    shard_cols = lax.all_gather(arrived, "tp", axis=1, tiled=True)
+    shard_cols = jnp.concatenate(
+        lax.all_to_all(jnp.stack([arrived] * lax.axis_size("tp")), "tp", 0, 0), axis=1
+    )
     gate_val = jnp.dot(shard_cols, gate_weight, preferred_element_type=jnp.float32)
     up_val = jnp.dot(shard_cols, up_weight, preferred_element_type=jnp.float32)
     hidden = (jax.nn.silu(gate_val) * up_val).astype(jnp.bfloat16)

time: 198 us -> 295 us (1.49)
  waiting for transfers between devices: 57.1 us -> 154 us
  blocking collectives: 79.7 us -> 72.7 us
  local copies, waits for them, and re-layouts: 7.53 us -> 11 us
  starting transfers between devices: 12.3 us -> 15.7 us
    all_to_all x0 -> x1, waiting for transfers between devices: none -> 140 us  [per_device(): lax.all_to_all(jnp.stack([arrived] * lax.axis_size('tp')), 'tp', 0, 0)]
    all_gather x1 -> x0, waiting for transfers between devices: 44 us -> none  [per_device(): shard_cols = lax.all_gather(arrived, 'tp', axis=1, tiled=True)]
    all_to_all x1, waiting for transfers between devices: 1.29 us -> 13.2 us  [per_device(): lax.all_to_all(expert_result, 'ep', split_axis=0, concat_axis=0, tiled=True)]
    reduce_scatter x1, waiting for transfers between devices: 11.8 us -> 0.02 us  [in_one_piece(): lax.psum_scatter(both, axis, scatter_dimension=dim, tiled=True)]
    all_to_all x0 -> x1, starting transfers between devices: none -> 9.66 us  [per_device(): lax.all_to_all(jnp.stack([arrived] * lax.axis_size('tp')), 'tp', 0, 0)]
    all_to_all x1, blocking collectives: 52.2 us -> 45.4 us  [sent_to_all(): lax.all_to_all(jnp.broadcast_to(x[None], (devices, *x.shape)), axis, 0, 0...]
    all_to_all x1, starting transfers between devices: 9.89 us -> 3.88 us  [per_device(): lax.all_to_all(expert_result, 'ep', split_axis=0, concat_axis=0, tiled=True)]
    another operation x1 -> x3, local copies, waits for them, and re-layouts: 0.01 us -> 3.43 us  [the longest x2 3.43 us: per_device(): jnp.stack([arrived] * lax.axis_size('tp'))]
  transfers between devices with their start and end apart: 4 -> 4, of which waited for: 3 -> 2; matrix products, arithmetic and copies ran while one was open for 11% -> 8% of each run, Pallas kernels for 0% -> 0%
where the time goes in v1:
time: 295 us; the launch traced here: 294 us
  waiting for transfers between devices  154 us (52%)
  blocking collectives  72.7 us (25%)
  matrix products  17.5 us (6%)
  starting transfers between devices  15.7 us (5%)
  between operations  14.3 us (5%)
  local copies, waits for them, and re-layouts  11 us (4%)
  other arithmetic  9.63 us (3%)
    all_to_all x1, waiting for transfers between devices, per_device(): lax.all_to_all(jnp.stack([arrived] * lax.axis_size('tp')), 'tp', 0, 0)  140 us
    all_to_all x1, blocking collectives, sent_to_all(): lax.all_to_all(jnp.broadcast_to(x[None], (devices, *x.shape)), axis, 0, 0...  45.4 us
    all_to_all x1, blocking collectives, per_device(): lax.all_to_all(my_slice, 'ep', split_axis=0, concat_axis=0, tiled=True)  27.3 us
    all_to_all x1, waiting for transfers between devices, per_device(): lax.all_to_all(expert_result, 'ep', split_axis=0, concat_axis=0, tiled=True)  13.2 us
    all_to_all x1, starting transfers between devices, per_device(): lax.all_to_all(jnp.stack([arrived] * lax.axis_size('tp')), 'tp', 0, 0)  9.66 us
  transfers between devices with their start and end apart: 4, of which 2 were waited for; matrix products, arithmetic and copies ran while one was open for 8% of the time, Pallas kernels for 0%

profile of v1, /device:TPU:1, one launch (start us, length us, event | category | flops | bytes accessed | tf_op | source)
XLA Modules:
  0.0 294.4 jit_solution(17946289315237139592)
XLA Ops:
  7.2 0.9 copy.28
  8.4 1.2 reduce-window.6
  10.8 1.5 convert_reduce_fusion
  12.7 2.0 fusion.13
  14.8 27.3 %all_to_all.31 = bf16[32,24,256]{2,1,0:T(8,128)(2,1)S(1)} all-to-all(bf16[32,24,256]{2,1,0:T(8,128)(2,1)S(1)} %bitcast.91), channel_id=1, replica_groups=mesh['ep'=32,'tp'=16] {'ep'}, dimensions={0} | all-to-all | bytes 786432 | tf_op jit(solution)/shard_map/all_to_all | solution.py:128
  42.3 3.3 %stack.5 = bf16[16,768,256]{1,2,0:T(8,128)(2,1)} broadcast(bf16[768,256]{0,1:T(8,128)(2,1)S(1)} %copy.32), dimensions={1,2} | broadcast | bytes 6684672 | tf_op jit(solution)/shard_map/stack | solution.py:130
  45.5 9.7 %all-to-all-start.1 = ((bf16[16,768,256]{1,2,0:T(8,128)(2,1)}), bf16[16,768,256]{1,2,0:T(8,128)(2,1)}, u32[]{:S(2)}, u32[]{:S(2)}) async-start(bf16[16,768,256]{1,2,0:T(8,128)(2,1)} %stack.5), calls=%async_computation.2 | async-start | bytes 12582912 | tf_op jit(solution)/shard_map/all_to_all | solution.py:130
  55.3 2.1 collective-permute-start
  58.5 2.4 convolution_convert_fusion.1
  61.7 3.2 %convolution_convert_fusion = bf16[256,4096]{1,0:T(8,128)(2,1)} fusion(bf16[128,4096]{1,0:T(8,128)(2,1)S(1)} %copy-done, f32[256,128]{1,0:T(8,128)S(1)} %convert_element_type.122, f32[15,128]{1,0:T(8,128)S(1)} %convert_element_type.124, f32[128]{0:T(128)S(1)} %dynamic_slice.10, f32[256]{0:T(256)S(1)} %get-tuple-element.18, f32[128]{0:T(128)} %get-tuple-element.14, ...), kind=kOutput, calls=%fused_computation.4 | convolution fusion | flops 279379968 | bytes 3323908 | tf_op jit(solution)/shard_map/dot_general | solution.py:74
  65.0 3.5 %pad_maximum_fusion = bf16[384,4096]{1,0:T(8,128)(2,1)} fusion(bf16[128,4096]{1,0:T(8,128)(2,1)S(1)} %convolution_convert_fusion.1, bf16[256,4096]{1,0:T(8,128)(2,1)} %convolution_convert_fusion), kind=kLoop, calls=%fused_computation.6 | loop fusion | flops 6291456 | bytes 6291456 | tf_op jit(solution)/shard_map/concatenate | solution.py:34
  68.5 140.3 %all-to-all-done.1 = bf16[16,768,256]{1,2,0:T(8,128)(2,1)} async-done(((bf16[16,768,256]{1,2,0:T(8,128)(2,1)}), bf16[16,768,256]{1,2,0:T(8,128)(2,1)}, u32[]{:S(2)}, u32[]{:S(2)}) %all-to-all-start.1) | async-done | bytes 6291488 | tf_op jit(solution)/shard_map/all_to_all | solution.py:130
  208.8 4.0 %fusion.11 = f32[768,64]{0,1:T(8,128)S(1)} fusion(bf16[768,4096]{0,1:T(8,128)(2,1)} %bitcast.13, bf16[1,4096,64]{1,2,0:T(8,128)(2,1)S(1)} %copy-done.3), kind=kOutput, calls=%fused_computation.39 | convolution fusion | flops 402653184 | bytes 7012352 | tf_op jit(solution)/shard_map/dot_general | solution.py:132
  212.8 4.0 %fusion.5 = bf16[768,64]{0,1:T(8,128)(2,1)S(1)} fusion(bf16[768,4096]{0,1:T(8,128)(2,1)} %bitcast.13, bf16[1,4096,64]{1,2,0:T(8,128)(2,1)S(1)} %copy-done.2, f32[768,64]{0,1:T(8,128)S(1)} %fusion.11), kind=kOutput, calls=%fused_computation.16 | convolution fusion | flops 402948096 | bytes 7110656 | tf_op jit(solution)/shard_map/dot_general | solution.py:133
  217.0 45.4 %all_to_all.32 = bf16[16,768,64]{1,2,0:T(8,128)(2,1)S(1)} all-to-all(bf16[16,768,64]{1,2,0:T(8,128)(2,1)S(1)} %broadcast_in_dim.2), channel_id=1, replica_groups=mesh['ep'=32,'tp'=16] {'tp'}, dimensions={0} | all-to-all | bytes 3145728 | tf_op jit(solution)/shard_map/all_to_all | solution.py:19
  262.4 1.4 convolution_convert_fusion.2
  263.8 3.9 %all-to-all-start.3 = ((bf16[32,24,256]{2,1,0:T(8,128)(2,1)}), bf16[32,24,256]{2,1,0:T(8,128)(2,1)S(1)}, u32[]{:S(2)}, u32[]{:S(2)}) async-start(bf16[32,24,256]{2,1,0:T(8,128)(2,1)} %bitcast.20), calls=%async_computation.4 | async-start | bytes 786432 | tf_op jit(solution)/shard_map/all_to_all | solution.py:138
  267.8 1.6 slice.152
  269.3 13.2 %all-to-all-done.3 = bf16[32,24,256]{2,1,0:T(8,128)(2,1)S(1)} async-done(((bf16[32,24,256]{2,1,0:T(8,128)(2,1)}), bf16[32,24,256]{2,1,0:T(8,128)(2,1)S(1)}, u32[]{:S(2)}, u32[]{:S(2)}) %all-to-all-start.3) | async-done | bytes 393248 | tf_op jit(solution)/shard_map/all_to_all | solution.py:138
  282.6 0.8 gather_fusion
  283.4 0.8 gather_fusion.1
  284.3 0.8 gather_fusion.2
  285.1 0.8 gather_fusion.3
  286.0 1.6 add_convert_fusion.2
  (53 shorter events, 4.3 us)
Async XLA Ops:
  7.2 54.6 %copy-start = (bf16[128,4096]{1,0:T(8,128)(2,1)S(1)}, bf16[128,4096]{1,0:T(8,128)(2,1)}, u32[]{:S(2)}) copy-start(bf16[128,4096]{1,0:T(8,128)(2,1)} %param.17) | copy-start | bytes 3145732
  7.2 5.1 %copy-start.1 = (bf16[128,4096]{1,0:T(8,128)(2,1)S(1)}, bf16[128,4096]{1,0:T(8,128)(2,1)}, u32[]{:S(2)}) copy-start(bf16[128,4096]{1,0:T(8,128)(2,1)} %param.18) | copy-start | bytes 3145732
  7.2 5.5 %copy-start.6 = (f32[4096]{0:T(1024)S(1)}, f32[4096]{0:T(1024)}, u32[]{:S(2)}) copy-start(f32[4096]{0:T(1024)} %param.19) | copy-start | bytes 49156
  45.5 9.7 %copy-start.5 = (bf16[256,128]{1,0:T(8,128)(2,1)S(1)}, bf16[256,128]{1,0:T(8,128)(2,1)}, u32[]{:S(2)}) copy-start(bf16[256,128]{1,0:T(8,128)(2,1)} %param.14) | copy-start | bytes 196612
  45.5 12.4 %copy-start.9 = (bf16[4096,32]{0,1:T(8,128)(2,1)S(1)}, bf16[4096,32]{0,1:T(8,128)(2,1)}, u32[]{:S(2)}) copy-start(bf16[4096,32]{0,1:T(8,128)(2,1)} %param.25) | copy-start | bytes 786436
  45.5 163.3 %all-to-all-start.1 = ((bf16[16,768,256]{1,2,0:T(8,128)(2,1)}), bf16[16,768,256]{1,2,0:T(8,128)(2,1)}, u32[]{:S(2)}, u32[]{:S(2)}) async-start(bf16[16,768,256]{1,2,0:T(8,128)(2,1)} %stack.5), calls=%async_computation.2 | async-start | bytes 12582912 | tf_op jit(solution)/shard_map/all_to_all | solution.py:130
  55.2 3.3 %copy-start.4 = (bf16[32,4096]{1,0:T(8,128)(2,1)S(1)}, bf16[32,4096]{1,0:T(8,128)(2,1)}, u32[]{:S(2)}) copy-start(bf16[32,4096]{1,0:T(8,128)(2,1)} %param.27) | copy-start | bytes 786436
  55.2 212.6 %reduce-scatter.2.cloned.1.call-start = ((), (), s32[]{:S(2)}) async-start(), calls=%async_computation.5 | async-start | bytes 3342336 | tf_op jit(solution)/shard_map/reduce_scatter | solution.py:35
  55.3 6.5 %collective-permute-start = (bf16[15,128]{1,0:T(8,128)(2,1)S(1)}, bf16[15,128]{1,0:T(8,128)(2,1)S(1)}, u32[]{:S(2)}, u32[]{:S(2)}) collective-permute-start(bf16[15,128]{1,0:T(8,128)(2,1)S(1)} %slice.88), channel_id=1, source_target_pairs={{0,16},{16,32},{32,48},{48,64},{64,80},{80,96},{96,112},{112,128},... | collective-permute-start | bytes 11528 | tf_op jit(solution)/shard_map/ppermute | solution.py:14
  68.5 140.3 %copy-start.3 = (bf16[1,4096,64]{1,2,0:T(8,128)(2,1)S(1)}, bf16[1,4096,64]{1,2,0:T(8,128)(2,1)}, u32[]{:S(2)}) copy-start(bf16[1,4096,64]{1,2,0:T(8,128)(2,1)} %param.22) | copy-start | bytes 1572868
  208.8 4.0 %copy-start.2 = (bf16[1,4096,64]{1,2,0:T(8,128)(2,1)S(1)}, bf16[1,4096,64]{1,2,0:T(8,128)(2,1)}, u32[]{:S(2)}) copy-start(bf16[1,4096,64]{1,2,0:T(8,128)(2,1)} %param.23) | copy-start | bytes 1572868
  216.8 45.6 %copy-start.8 = (bf16[1,1024,256]{2,1,0:T(8,128)(2,1)S(1)}, bf16[1,1024,256]{2,1,0:T(8,128)(2,1)}, u32[]{:S(2)}) copy-start(bf16[1,1024,256]{2,1,0:T(8,128)(2,1)} %param.24) | copy-start | bytes 1572868
  262.4 5.3 %copy-start.7 = (f32[128,4]{0,1:T(4,128)S(1)}, f32[128,4]{0,1:T(4,128)}, u32[]{:S(2)}) copy-start(f32[128,4]{0,1:T(4,128)} %param.21) | copy-start | bytes 6148
  263.8 18.8 %all-to-all-start.3 = ((bf16[32,24,256]{2,1,0:T(8,128)(2,1)}), bf16[32,24,256]{2,1,0:T(8,128)(2,1)S(1)}, u32[]{:S(2)}, u32[]{:S(2)}) async-start(bf16[32,24,256]{2,1,0:T(8,128)(2,1)} %bitcast.20), calls=%async_computation.4 | async-start | bytes 786432 | tf_op jit(solution)/shard_map/all_to_all | solution.py:138
Sparse Core Ops, SparseCore 0:
  68.6 139.9 reduce-scatter.1
